TPU v7x, 512 devices: a whole 4x4x16 slice. The times are simulated.
512 devices in a mesh: ep: 32 (over z, core), tp: 16 (over y, x).
Axes of the slice: x: 4, y: 4, z: 16, core: 2. Of those that a mesh axis runs over, the one named last changes fastest.
Arguments:
- mixer_input: bfloat16 [8192, 2048], P('ep'), may hold values from -6 to 6
- mixer_gain: float32 [2048], replicated, may hold values from 0.1 to 1.9
- query_weight: bfloat16 [2048, 2048], P(None, 'tp'), may hold values from -0.13258252 to 0.13258252
- key_weight: bfloat16 [2048, 1024], P(None, 'tp'), may hold values from -2.78423295 to 2.78423295
- value_weight: bfloat16 [2048, 1024], P(None, 'tp'), may hold values from -0.125 to 0.125
- output_weight: bfloat16 [2048, 2048], P(None, 'tp'), may hold values from -1 to 1
- sink_logit: float32 [32], P('tp'), may hold values from 2 to 7
- expert_input: bfloat16 [4096, 2048], P('ep'), may hold values from -6 to 6
- expert_gain: float32 [2048], replicated, may hold values from 0.1 to 1.9
- routes: int32 [4096, 4], P('ep'), may hold values from 0 to 31, all different within a row; in each aligned block of 128 rows (0 to 127, 128 to 255, ...) at most 32 rows name the same one
- route_logits: float32 [4096, 4], P('ep'), may hold values from -6 to 6
- gate_weight: bfloat16 [32, 2048, 2048], P('ep', None, 'tp'), may hold values from -0.375 to 0.375
- up_weight: bfloat16 [32, 2048, 2048], P('ep', None, 'tp'), may hold values from -0.375 to 0.375
- down_weight: bfloat16 [32, 2048, 2048], P('ep', None, 'tp'), may hold values from -0.03125 to 0.03125
Outputs:
- mixer_output: bfloat16 [8192, 2048], P('ep', 'tp')
- expert_output: bfloat16 [4096, 2048], P('ep', 'tp')
Inputs may be any that keep to these rules, and one draw needn't show every extreme that they name: `routes`: each token names 4 different experts. Among the 128 tokens of one index of ep (aligned blocks) no expert is named more than 32 times, and in some blocks one expert is named exactly 32 times.
All inputs are finite; a program needn't handle non-finite values.
Results may differ from a plain program's by a relative error of at most 0.0055.
The roundings to bfloat16 on the way count: a program that leaves them out, or rounds other values in their place, can miss the bound.
Values may be sent and summed in bfloat16 or wider, within the bound.
No kernel may reach another device: no remote copies, remote signals or barrier semaphores. Data moves between devices by JAX's collectives and lax.ppermute only.
A program may use at most 64 MiB of HBM per device.

v0:
```python
import jax
import jax.numpy as jnp
from jax import lax
from jax.sharding import Mesh
from jax.sharding import PartitionSpec as P

HEAD_DIM = 64
TOP_K = 4
WINDOW = 128
GRID_W = 64
EP = ("ep_0", "ep_1")


EPSILON = 1e-06
LIMIT = 7.0
SLOPE = 1.702
BASE = 10000.0


def extended(shard, sides, width):
    for axis, dim in sides:
        devices, length = (lax.axis_size(axis), shard.shape[dim])
        up = [(i, (i + 1) % devices) for i in range(devices - 1)]
        down = [(j, i) for i, j in up]
        last = lax.slice_in_dim(shard, length - width, length, axis=dim)
        first = lax.slice_in_dim(shard, 0, width, axis=dim)
        before = lax.ppermute(last, axis, up)
        after = lax.ppermute(first, axis, down)
        shard = jnp.concatenate([before, shard, after], axis=dim)
    return shard


def cut_along(shard, dim, devices):
    shape = shard.shape
    pieces = shard.reshape(*shape[:dim], devices, shape[dim] // devices, *shape[dim + 1 :])
    return jnp.moveaxis(pieces, dim, 0)


def joined_along(pieces, dim):
    pieces = jnp.moveaxis(pieces, 0, dim)
    shape = pieces.shape
    return pieces.reshape(*shape[:dim], shape[dim] * shape[dim + 1], *shape[dim + 2 :])


def exchange_in_order(pieces, axes, order):
    inside = pieces.shape[1:]
    whole = pieces.reshape(*(lax.axis_size(a) for a in axes), *inside)
    for k in order:
        whole = lax.all_to_all(whole, axes[k], k, k, tiled=True)
    return whole.reshape(-1, *inside)


def exchange_by_chip(shard, groups, order, split_dim, concat_dim):
    devices = lax.axis_size(groups[0]) * lax.axis_size(groups[1])
    pieces = cut_along(shard, split_dim, devices)
    return joined_along(exchange_in_order(pieces, groups, order), concat_dim)


def side_by_side(arrays, axis, dim, along):
    widths = [a.shape[along] for a in arrays]
    both = jnp.concatenate(arrays, axis=along)
    whole = lax.all_gather(both, axis, axis=dim, tiled=True)
    return tuple(jnp.split(whole, [sum(widths[:k]) for k in range(1, len(widths))], axis=along))


def normalize(rows, gain):
    values = rows.astype(jnp.float32)
    scaled = values * lax.rsqrt(jnp.mean(values * values, axis=-1, keepdims=True) + EPSILON)
    return (scaled * gain).astype(jnp.bfloat16)


def turn(values, cosine, sine):
    first, second = jnp.split(values, 2, axis=-1)
    cosine = cosine[:, None, :]
    sine = sine[:, None, :]
    return jnp.concatenate(
        [first * cosine - second * sine, second * cosine + first * sine], axis=-1
    )


def axial_rope(values, places):
    quarter = values.shape[-1] // 4
    frequency = BASE ** (-jnp.arange(quarter, dtype=jnp.float32) / quarter)
    row_angle = (places // GRID_W).astype(jnp.float32)[:, None] * frequency[None, :]
    column_angle = (places % GRID_W).astype(jnp.float32)[:, None] * frequency[None, :]
    row_part, column_part = jnp.split(values, 2, axis=-1)
    return jnp.concatenate(
        [
            turn(row_part, jnp.cos(row_angle), jnp.sin(row_angle)),
            turn(column_part, jnp.cos(column_angle), jnp.sin(column_angle)),
        ],
        axis=-1,
    )


def activate(gate, up):
    capped = jnp.minimum(gate, LIMIT)
    bounded = jnp.clip(up, -LIMIT, LIMIT)
    return (capped * jax.nn.sigmoid(SLOPE * capped) * (bounded + 1.0)).astype(jnp.bfloat16)


def add_product(piece, weight):
    return jnp.dot(piece, weight, preferred_element_type=jnp.float32)


def shards(
    mixer_input,
    mixer_gain,
    query_weight,
    key_weight,
    value_weight,
    output_weight,
    sink_logit,
    expert_input,
    expert_gain,
    routes,
    route_logits,
    gate_weight,
    up_weight,
    down_weight,
):
    tokens = mixer_input.shape[0]
    query_heads = query_weight.shape[1] // HEAD_DIM
    key_heads = key_weight.shape[1] // HEAD_DIM
    group = query_heads // key_heads
    blocks = tokens // WINDOW
    offset = lax.axis_index(EP) * tokens
    length = lax.axis_size(EP) * tokens
    places = offset + jnp.arange(tokens, dtype=jnp.int32)
    normed = normalize(mixer_input, mixer_gain)
    query = jnp.dot(normed, query_weight, preferred_element_type=jnp.float32).reshape(
        tokens, query_heads, HEAD_DIM
    )
    query = (
        axial_rope(query, places)
        .astype(jnp.bfloat16)
        .reshape(blocks, WINDOW, key_heads, group, HEAD_DIM)
    )
    keys = jnp.dot(normed, key_weight, preferred_element_type=jnp.float32).reshape(
        tokens, key_heads, HEAD_DIM
    )
    keys = axial_rope(keys, places).astype(jnp.bfloat16).reshape(tokens, key_heads * HEAD_DIM)
    values = jnp.dot(normed, value_weight, preferred_element_type=jnp.float32).astype(jnp.bfloat16)
    stacked = jnp.concatenate([keys, values], axis=1)
    widened = extended(stacked, ((EP, 0),), WINDOW)
    framed = widened.reshape(blocks + 2, WINDOW, 2, key_heads, HEAD_DIM)
    nearby = jnp.concatenate([framed[:-2], framed[1:-1], framed[2:]], axis=1)
    scores = jnp.einsum(
        "nqgrd,nkgd->ngrqk", query, nearby[:, :, 0], preferred_element_type=jnp.float32
    ) * HEAD_DIM ** (-0.5)
    query_place = places.reshape(blocks, WINDOW)
    key_place = (
        offset
        + (jnp.arange(blocks, dtype=jnp.int32)[:, None] - 1) * WINDOW
        + jnp.arange(3 * WINDOW, dtype=jnp.int32)[None, :]
    )
    allowed = (
        (jnp.abs(query_place[:, :, None] - key_place[:, None, :]) <= WINDOW)
        & (key_place[:, None, :] >= 0)
        & (key_place[:, None, :] < length)
    )
    scores = jnp.where(allowed[:, None, None], scores, -1e30)
    sinks = sink_logit.reshape(key_heads, group)[None, :, :, None]
    top = jnp.maximum(jnp.max(scores, axis=-1), sinks)
    weights = jnp.exp(scores - top[..., None])
    denominator = jnp.sum(weights, axis=-1) + jnp.exp(sinks - top)
    shares = (weights / denominator[..., None]).astype(jnp.bfloat16)
    mixed = jnp.einsum(
        "ngrqk,nkgd->nqgrd", shares, nearby[:, :, 1], preferred_element_type=jnp.float32
    )
    mixed = mixed.astype(jnp.bfloat16).reshape(tokens, query_heads * HEAD_DIM)
    experts = lax.axis_size(EP)
    rows_here = expert_input.shape[0]
    capacity = 2 * rows_here * TOP_K // experts
    expert_normed = normalize(expert_input, expert_gain)
    chances = jax.nn.softmax(route_logits, axis=-1)
    chosen = routes.reshape(-1)
    marks = (chosen[:, None] == jnp.arange(experts, dtype=jnp.int32)[None, :]).astype(jnp.int32)
    earlier = jnp.sum((jnp.cumsum(marks, axis=0) - marks) * marks, axis=1)
    target = chosen * capacity + earlier
    source = (
        jnp.full((experts * capacity,), rows_here, jnp.int32)
        .at[target]
        .set(jnp.arange(chosen.shape[0], dtype=jnp.int32) // TOP_K)
    )
    padded = jnp.concatenate(
        [expert_normed, jnp.zeros((1, expert_normed.shape[1]), jnp.bfloat16)], axis=0
    )
    down_local = down_weight[0]
    gate_local = gate_weight[0]
    up_local = up_weight[0]
    width = padded.shape[1] // lax.axis_size("tp")
    own = lax.dynamic_slice_in_dim(padded, lax.axis_index("tp") * width, width, 1)
    outgoing = own[source].reshape(experts, capacity, width)
    received = lax.all_to_all(outgoing, EP, split_axis=0, concat_axis=0, tiled=True)
    flat = received.reshape(experts * capacity, width)
    head_piece, feature_piece = side_by_side((mixed, flat), "tp", 1, 0)
    mixer_total = add_product(head_piece, output_weight)
    gate = add_product(feature_piece, gate_local)
    up = add_product(feature_piece, up_local)
    hidden = activate(gate, up)
    result = add_product(lax.all_gather(hidden, "tp", axis=1, tiled=True), down_local)
    result = result.astype(jnp.bfloat16).reshape(experts, capacity, down_local.shape[1])
    returned = exchange_by_chip(result, ("ep_0", "ep_1"), (1, 0), 0, 0)
    mixer_output = mixer_total.astype(jnp.bfloat16)
    results = returned.reshape(experts * capacity, returned.shape[2])
    picked = results[target].astype(jnp.float32).reshape(rows_here, TOP_K, returned.shape[2])
    expert_output = jnp.sum(picked * chances[:, :, None], axis=1).astype(jnp.bfloat16)
    return (mixer_output, expert_output)


def solution(mesh):
    finer = Mesh(mesh.devices.reshape(16, 2, mesh.shape["tp"]), ("ep_0", "ep_1", "tp"))
    in_specs = (
        P(EP, None),
        P(),
        P(None, "tp"),
        P(None, "tp"),
        P(None, "tp"),
        P(None, "tp"),
        P("tp"),
        P(EP, None),
        P(),
        P(EP, None),
        P(EP, None),
        P(EP, None, "tp"),
        P(EP, None, "tp"),
        P(EP, None, "tp"),
    )
    out_specs = (P(EP, "tp"), P(EP, "tp"))
    return jax.shard_map(
        shards, mesh=finer, in_specs=in_specs, out_specs=out_specs, check_vma=False
    )
```

profile of v0, /device:TPU:1, one launch (start us, length us, event | category | flops | bytes accessed | tf_op | source)
XLA Modules:
  0.0 251.5 jit_solution(9797498149042853800)
XLA Ops:
  7.2 0.7 broadcast_multiply_fusion
  7.9 0.8 copy.46
  8.7 0.1 eq.28
  8.8 0.1 eq.32
  8.9 1.2 fusion.26
  10.2 0.1 copy.45
  10.3 0.1 mul.314
  10.4 1.2 reduce-window.6
  11.6 0.2 slice_reduce_fusion
  11.9 0.1 fusion.40
  12.0 2.4 scatter_custom_fusion
  14.5 1.3 fusion.28
  15.8 4.3 %gather_fusion = bf16[1024,128]{1,0:T(8,128)(2,1)} fusion(bf16[129,128]{1,0:T(8,128)(2,1)S(1)} %pad_dynamic-slice_fusion, s32[1024]{0:T(1024)S(1)} %fusion.69), kind=kCustom, calls=%fused_computation | custom fusion | bytes 528384 | tf_op jit(solution)/shard_map/gather | solution.py:194
  20.1 16.9 %all-to-all-start = ((bf16[32,32,128]{2,1,0:T(8,128)(2,1)}), bf16[32,32,128]{2,1,0:T(8,128)(2,1)S(1)}, u32[]{:S(2)}, u32[]{:S(2)}) async-start(bf16[32,32,128]{2,1,0:T(8,128)(2,1)} %bitcast.20), calls=%async_computation | async-start | bytes 524288 | tf_op jit(solution)/shard_map/all_to_all | solution.py:195
  37.1 0.3 fusion.4
  37.4 0.5 convolution_bitcast_fusion
  37.9 0.1 constant_dynamic-update-slice_fusion.3
  38.1 0.1 constant_dynamic-update-slice_fusion.2
  38.2 0.1 constant_dynamic-update-slice_fusion.1
  38.4 0.1 constant_dynamic-update-slice_fusion
  38.5 0.5 fusion.25
  39.0 2.1 collective-permute-start.1
  41.2 3.4 %collective-permute-start = (bf16[128,128]{0,1:T(8,128)(2,1)S(1)}, bf16[128,128]{0,1:T(8,128)(2,1)S(1)}, u32[]{:S(2)}, u32[]{:S(2)}) collective-permute-start(bf16[128,128]{0,1:T(8,128)(2,1)S(1)} %get-tuple-element.11), channel_id=1, source_target_pairs={{0,16},{16,32},{32,48},{48,64},{64,80},{80,96},{96,112},{112,128},... | collective-permute-start | bytes 98312 | tf_op jit(solution)/shard_map/ppermute | solution.py:27
  44.6 0.2 multiply_cosine_fusion.1
  45.0 0.6 fusion.83
  45.6 0.5 fusion.36
  46.2 3.9 %collective-permute-done.1 = bf16[128,128]{0,1:T(8,128)(2,1)S(1)} collective-permute-done((bf16[128,128]{0,1:T(8,128)(2,1)S(1)}, bf16[128,128]{0,1:T(8,128)(2,1)S(1)}, u32[]{:S(2)}, u32[]{:S(2)}) %collective-permute-start.1) | collective-permute-done | bytes 32800 | tf_op jit(solution)/shard_map/ppermute | solution.py:28
  50.2 0.3 fusion.88
  50.7 0.1 fusion.30
  50.9 0.3 fusion.24
  51.1 0.1 copy.56
  51.3 0.1 reshape.520
  51.4 7.7 %all-to-all-done = bf16[32,32,128]{2,1,0:T(8,128)(2,1)S(1)} async-done(((bf16[32,32,128]{2,1,0:T(8,128)(2,1)}), bf16[32,32,128]{2,1,0:T(8,128)(2,1)S(1)}, u32[]{:S(2)}, u32[]{:S(2)}) %all-to-all-start) | async-done | bytes 262176 | tf_op jit(solution)/shard_map/all_to_all | solution.py:195
  59.1 0.7 pad_maximum_fusion
  59.9 69.0 %all-gather.3.cloned.1.call-done = bf16[1280,2048]{1,0:T(8,128)(2,1)} async-done(((bf16[1280,128]{1,0:T(8,128)(2,1)}), bf16[1280,2048]{1,0:T(8,128)(2,1)}) %all-gather.3.cloned.1.call-update) | async-done | bytes 5242896 | tf_op jit(solution)/shard_map/all_gather | solution.py:62
  128.9 3.6 %fusion.8 = f32[1024,128]{1,0:T(8,128)S(1)} fusion(bf16[1280,2048]{1,0:T(8,128)(2,1)} %all-gather.3.cloned.1.call-done, bf16[1,2048,128]{2,1,0:T(8,128)(2,1)S(1)} %copy-done), kind=kOutput, calls=%fused_computation.16 | convolution fusion | flops 537001984 | bytes 5242880 | tf_op jit(solution)/shard_map/dot_general | solution.py:103
  132.5 0.1 copy-done.4
  132.6 2.0 fusion.21
  134.6 71.7 %all-gather.5.cloned.1.call-done = bf16[1024,2048]{1,0:T(8,128)(2,1)} async-done(((bf16[1024,128]{1,0:T(8,128)(2,1)}), bf16[1024,2048]{1,0:T(8,128)(2,1)}) %all-gather.5.cloned.1.call-update) | async-done | bytes 4194320 | tf_op jit(solution)/shard_map/all_gather | solution.py:202
  206.4 3.4 %convolution_convert_fusion = bf16[1024,128]{1,0:T(8,128)(2,1)S(1)} fusion(bf16[1024,2048]{1,0:T(8,128)(2,1)} %all-gather.5.cloned.1.call-done, bf16[1,2048,128]{2,1,0:T(8,128)(2,1)S(1)} %copy-done.7), kind=kOutput, calls=%fused_computation.22 | convolution fusion | flops 537001984 | bytes 4980736 | tf_op jit(solution)/shard_map/dot_general | solution.py:103
  209.9 5.7 %all_to_all.15 = bf16[16,2,1,32,128]{4,3,0,2,1:T(8,128)(2,1)S(1)} all-to-all(bf16[16,2,1,32,128]{4,3,0,2,1:T(8,128)(2,1)S(1)} %copy.50), channel_id=1, replica_groups=mesh['ep_0'=16,'ep_1'=2,'tp'=16] {'ep_1'}, dimensions={1} | all-to-all | bytes 524288 | tf_op jit(solution)/shard_map/all_to_all | solution.py:49
  215.6 0.7 copy.51
  216.4 12.0 %all-to-all-start.2 = ((bf16[16,2,1,32,128]{4,3,1,2,0:T(8,128)(2,1)}), bf16[16,2,1,32,128]{4,3,1,2,0:T(8,128)(2,1)S(1)}, u32[]{:S(2)}, u32[]{:S(2)}) async-start(bf16[16,2,1,32,128]{4,3,1,2,0:T(8,128)(2,1)} %copy.51), calls=%async_computation.2 | async-start | bytes 524288 | tf_op jit(solution)/shard_map/all_to_all | solution.py:49
  228.4 0.1 copy.52
  228.6 2.3 convolution_convert_fusion.1
  230.9 11.5 %all-to-all-done.2 = bf16[16,2,1,32,128]{4,3,1,2,0:T(8,128)(2,1)S(1)} async-done(((bf16[16,2,1,32,128]{4,3,1,2,0:T(8,128)(2,1)}), bf16[16,2,1,32,128]{4,3,1,2,0:T(8,128)(2,1)S(1)}, u32[]{:S(2)}, u32[]{:S(2)}) %all-to-all-start.2) | async-done | bytes 262176 | tf_op jit(solution)/shard_map/all_to_all | solution.py:49
  242.4 1.3 gather_fusion.1
  243.7 0.9 fusion.37
  (63 shorter events, 0.9 us)
Async XLA Ops:
  7.2 121.7 %copy-start = (bf16[1,2048,128]{2,1,0:T(8,128)(2,1)S(1)}, bf16[1,2048,128]{2,1,0:T(8,128)(2,1)}, u32[]{:S(2)}) copy-start(bf16[1,2048,128]{2,1,0:T(8,128)(2,1)} %param.25) | copy-start | bytes 1572868
  14.4 22.6 %copy-start.1 = (bf16[256,2048]{1,0:T(8,128)(2,1)S(1)}, bf16[256,2048]{1,0:T(8,128)(2,1)}, u32[]{:S(2)}) copy-start(bf16[256,2048]{1,0:T(8,128)(2,1)} %param.14) | copy-start | bytes 3145732
  15.8 21.6 %copy-start.9 = (bf16[2048,64]{0,1:T(8,128)(2,1)S(1)}, bf16[2048,64]{0,1:T(8,128)(2,1)}, u32[]{:S(2)}) copy-start(bf16[2048,64]{0,1:T(8,128)(2,1)} %param.17) | copy-start | bytes 786436
  15.8 21.6 %copy-start.11 = (f32[2048]{0:T(1024)S(1)}, f32[2048]{0:T(1024)}, u32[]{:S(2)}) copy-start(f32[2048]{0:T(1024)} %param.15) | copy-start | bytes 24580
  20.1 18.4 %copy-start.10 = (bf16[2048,64]{0,1:T(8,128)(2,1)S(1)}, bf16[2048,64]{0,1:T(8,128)(2,1)}, u32[]{:S(2)}) copy-start(bf16[2048,64]{0,1:T(8,128)(2,1)} %param.18) | copy-start | bytes 786436
  20.1 39.0 %all-to-all-start = ((bf16[32,32,128]{2,1,0:T(8,128)(2,1)}), bf16[32,32,128]{2,1,0:T(8,128)(2,1)S(1)}, u32[]{:S(2)}, u32[]{:S(2)}) async-start(bf16[32,32,128]{2,1,0:T(8,128)(2,1)} %bitcast.20), calls=%async_computation | async-start | bytes 524288 | tf_op jit(solution)/shard_map/all_to_all | solution.py:195
  37.0 91.9 %all-gather.3.cloned.1.call-start = ((), (), s32[]{:S(2)}) async-start(), calls=%async_computation.3 | async-start | bytes 5570560 | tf_op jit(solution)/shard_map/all_gather | solution.py:62
  37.4 7.6 %copy-start.5 = (bf16[2048,128]{1,0:T(8,128)(2,1)S(1)}, bf16[2048,128]{1,0:T(8,128)(2,1)}, u32[]{:S(2)}) copy-start(bf16[2048,128]{1,0:T(8,128)(2,1)} %param.16) | copy-start | bytes 1572868
  39.0 11.1 %collective-permute-start.1 = (bf16[128,128]{0,1:T(8,128)(2,1)S(1)}, bf16[128,128]{0,1:T(8,128)(2,1)S(1)}, u32[]{:S(2)}, u32[]{:S(2)}) collective-permute-start(bf16[128,128]{0,1:T(8,128)(2,1)S(1)} %get-tuple-element.10), channel_id=1, source_target_pairs={{16,0},{32,16},{48,32},{64,48},{80,64},{96,80},{112,96},{128,112},... | collective-permute-start | bytes 98312 | tf_op jit(solution)/shard_map/ppermute | solution.py:28
  41.2 8.9 %collective-permute-start = (bf16[128,128]{0,1:T(8,128)(2,1)S(1)}, bf16[128,128]{0,1:T(8,128)(2,1)S(1)}, u32[]{:S(2)}, u32[]{:S(2)}) collective-permute-start(bf16[128,128]{0,1:T(8,128)(2,1)S(1)} %get-tuple-element.11), channel_id=1, source_target_pairs={{0,16},{16,32},{32,48},{48,64},{64,80},{80,96},{96,112},{112,128},... | collective-permute-start | bytes 98312 | tf_op jit(solution)/shard_map/ppermute | solution.py:27
  45.0 5.6 %copy-start.3 = (f32[2]{0:T(128)S(1)}, f32[2]{0:T(128)}, u32[]{:S(2)}) copy-start(f32[2]{0:T(128)} %param.20) | copy-start | bytes 28
  59.8 72.6 %copy-start.6 = (bf16[1,2048,128]{2,1,0:T(8,128)(2,1)S(1)}, bf16[1,2048,128]{2,1,0:T(8,128)(2,1)}, u32[]{:S(2)}) copy-start(bf16[1,2048,128]{2,1,0:T(8,128)(2,1)} %param.26) | copy-start | bytes 1572868
  59.9 146.5 %all-gather.5.cloned.1.call-start = ((), (), s32[]{:S(2)}) async-start(), calls=%async_computation.4 | async-start | bytes 4456448 | tf_op jit(solution)/shard_map/all_gather | solution.py:202
  128.9 3.7 %copy-start.4 = (bf16[1280,2048]{1,0:T(8,128)(2,1)S(1)}, bf16[1280,2048]{1,0:T(8,128)(2,1)}, u32[]{:S(2)}) copy-start(bf16[1280,2048]{1,0:T(8,128)(2,1)} %all-gather.3.cloned.1.call-done) | copy-start | bytes 15728644
  132.6 73.7 %copy-start.7 = (bf16[1,2048,128]{2,1,0:T(8,128)(2,1)S(1)}, bf16[1,2048,128]{2,1,0:T(8,128)(2,1)}, u32[]{:S(2)}) copy-start(bf16[1,2048,128]{2,1,0:T(8,128)(2,1)} %param.27) | copy-start | bytes 1572868
  209.8 18.6 %copy-start.2 = (f32[128,4]{0,1:T(4,128)S(1)}, f32[128,4]{0,1:T(4,128)}, u32[]{:S(2)}) copy-start(f32[128,4]{0,1:T(4,128)} %param.24) | copy-start | bytes 6148
  209.8 18.7 %copy-start.8 = (bf16[2048,128]{1,0:T(8,128)(2,1)S(1)}, bf16[2048,128]{1,0:T(8,128)(2,1)}, u32[]{:S(2)}) copy-start(bf16[2048,128]{1,0:T(8,128)(2,1)} %param.19) | copy-start | bytes 1572868
  216.4 26.0 %all-to-all-start.2 = ((bf16[16,2,1,32,128]{4,3,1,2,0:T(8,128)(2,1)}), bf16[16,2,1,32,128]{4,3,1,2,0:T(8,128)(2,1)S(1)}, u32[]{:S(2)}, u32[]{:S(2)}) async-start(bf16[16,2,1,32,128]{4,3,1,2,0:T(8,128)(2,1)} %copy.51), calls=%async_computation.2 | async-start | bytes 524288 | tf_op jit(solution)/shard_map/all_to_all | solution.py:49
Sparse Core Ops, SparseCore 0:
  60.0 68.8 all-gather.2
  134.8 71.5 all-gather.4
where the time goes:
time: 255 us; the launch traced here: 251 us
  waiting for transfers between devices  164 us (64%)
  starting transfers between devices  34.5 us (14%)
  between operations  14.5 us (6%)
  matrix products  13.4 us (5%)
  local copies, waits for them, and re-layouts  11 us (4%)
  other arithmetic  8.37 us (3%)
  blocking collectives  5.75 us (2%)
    all_gather x1, waiting for transfers between devices, shards(): lax.all_gather(hidden, 'tp', axis=1, tiled=True)  71.7 us
    all_gather x1, waiting for transfers between devices, side_by_side(): whole = lax.all_gather(both, axis, axis=dim, tiled=True)  69 us
    all_to_all x1, starting transfers between devices, shards(): lax.all_to_all(outgoing, EP, split_axis=0, concat_axis=0, tiled=True)  16.9 us
    all_to_all x1, starting transfers between devices, exchange_in_order(): whole = lax.all_to_all(whole, axes[k], k, k, tiled=True)  12 us
    all_to_all x1, waiting for transfers between devices, exchange_in_order(): whole = lax.all_to_all(whole, axes[k], k, k, tiled=True)  11.5 us
    dot_general x4, matrix products, add_product(): return jnp.dot(piece, weight, preferred_element_type=jnp.float32)  11.3 us
    all_to_all x1, waiting for transfers between devices, shards(): lax.all_to_all(outgoing, EP, split_axis=0, concat_axis=0, tiled=True)  7.68 us
    all_to_all x1, blocking collectives, exchange_in_order(): whole = lax.all_to_all(whole, axes[k], k, k, tiled=True)  5.75 us
  transfers between devices with their start and end apart: 6, of which 5 were waited for; matrix products, arithmetic and copies ran while one was open for 3% of the time, Pallas kernels for 0%

commit v1 on v0

v1 whole, which is shorter than its diff:
```python
import jax
import jax.numpy as jnp
from jax import lax
from jax.experimental import pallas as pl
from jax.experimental.pallas import tpu as pltpu
from jax.sharding import Mesh
from jax.sharding import PartitionSpec as P

HEAD_DIM = 64
TOP_K = 4
WINDOW = 128
GRID_W = 64
EP = ("ep_0", "ep_1")
TP = ("y", "x")

EPSILON = 1e-06
LIMIT = 7.0
SLOPE = 1.702
BASE = 10000.0


def extended(shard, axis, width):
    devices, length = lax.axis_size(axis), shard.shape[0]
    up = [(i, (i + 1) % devices) for i in range(devices - 1)]
    down = [(j, i) for i, j in up]
    before = lax.ppermute(shard[length - width :], axis, up)
    after = lax.ppermute(shard[:width], axis, down)
    return jnp.concatenate([before, shard, after], axis=0)


def swap(pieces, axis):
    return lax.all_to_all(pieces, axis, 0, 0, tiled=True)


def spread(shard, axis):
    return swap(jnp.broadcast_to(shard[None], (lax.axis_size(axis), *shard.shape)), axis)


def normalize(rows, gain):
    values = rows.astype(jnp.float32)
    scaled = values * lax.rsqrt(jnp.mean(values * values, axis=-1, keepdims=True) + EPSILON)
    return (scaled * gain).astype(jnp.bfloat16)


def turn(values, cosine, sine):
    first, second = jnp.split(values, 2, axis=-1)
    cosine = cosine[:, None, :]
    sine = sine[:, None, :]
    return jnp.concatenate(
        [first * cosine - second * sine, second * cosine + first * sine], axis=-1
    )


def axial_rope(values, places):
    quarter = values.shape[-1] // 4
    frequency = BASE ** (-jnp.arange(quarter, dtype=jnp.float32) / quarter)
    row_angle = (places // GRID_W).astype(jnp.float32)[:, None] * frequency[None, :]
    column_angle = (places % GRID_W).astype(jnp.float32)[:, None] * frequency[None, :]
    row_part, column_part = jnp.split(values, 2, axis=-1)
    return jnp.concatenate(
        [
            turn(row_part, jnp.cos(row_angle), jnp.sin(row_angle)),
            turn(column_part, jnp.cos(column_angle), jnp.sin(column_angle)),
        ],
        axis=-1,
    )


def activate(gate, up):
    capped = jnp.minimum(gate, LIMIT)
    bounded = jnp.clip(up, -LIMIT, LIMIT)
    return (capped * jax.nn.sigmoid(SLOPE * capped) * (bounded + 1.0)).astype(jnp.bfloat16)


def dot(a, b):
    return jnp.dot(a, b, preferred_element_type=jnp.float32)


def dispatch(rows, gain, routes, place, experts, slots, width):
    tokens = rows.shape[0]
    capacity = slots * lax.axis_size("x")

    def kernel(place_ref, rows_ref, gain_ref, routes_ref, routes_t_ref, out_ref, target_ref):
        values = rows_ref[...].astype(jnp.float32)
        scale = lax.rsqrt(jnp.mean(values * values, axis=-1, keepdims=True) + EPSILON)
        start = pl.multiple_of(place_ref[0] * width, width)
        own = rows_ref[:, pl.ds(start, width)].astype(jnp.float32)
        normed = (own * scale * gain_ref[:, pl.ds(start, width)]).astype(jnp.bfloat16)
        first = lax.broadcasted_iota(jnp.int32, (tokens, tokens), 0)
        second = lax.broadcasted_iota(jnp.int32, (tokens, tokens), 1)
        expert = lax.broadcasted_iota(jnp.int32, (experts, tokens), 0)
        named = jnp.zeros((experts, tokens), jnp.float32)
        for k in range(TOP_K):
            named = named + (routes_t_ref[k : k + 1, :] == expert).astype(jnp.float32)
        earlier = dot(named.astype(jnp.bfloat16), (first < second).astype(jnp.bfloat16))
        rank = jnp.where(named > 0.0, earlier.astype(jnp.int32), -1) - place_ref[1] * slots
        slot = lax.broadcasted_iota(jnp.int32, (experts, slots, tokens), 1)
        chosen = (rank[:, None, :] == slot).astype(jnp.float32).reshape(experts * slots, tokens)
        out_ref[...] = dot(chosen.astype(jnp.bfloat16), normed).astype(jnp.bfloat16)
        column = lax.broadcasted_iota(jnp.int32, (tokens, experts), 1)
        marks = [(routes_ref[:, k : k + 1] == column).astype(jnp.float32) for k in range(TOP_K)]
        before = dot((second < first).astype(jnp.bfloat16), sum(marks).astype(jnp.bfloat16))
        position = before + column.astype(jnp.float32) * float(capacity)
        target_ref[...] = jnp.concatenate(
            [jnp.sum(mark * position, axis=1, keepdims=True) for mark in marks], axis=1
        ).astype(jnp.int32)

    vmem = pl.BlockSpec(memory_space=pltpu.VMEM)
    return pl.pallas_call(
        kernel,
        out_shape=(
            jax.ShapeDtypeStruct((experts * slots, width), jnp.bfloat16),
            jax.ShapeDtypeStruct((tokens, TOP_K), jnp.int32),
        ),
        in_specs=[pl.BlockSpec(memory_space=pltpu.SMEM)] + [vmem] * 4,
        out_specs=(vmem, vmem),
        name="dispatch",
    )(place, rows, gain[None, :], routes, routes.T)


def gated(rows, weights):
    parts, n, k = rows.shape
    pieces, _, both = weights.shape
    u = both // 2

    def kernel(rows_ref, weights_ref, out_ref):
        total = dot(rows_ref[0], weights_ref[0, :k, :])
        for part in range(1, parts):
            total = total + dot(rows_ref[part], weights_ref[0, part * k : (part + 1) * k, :])
        hidden = activate(total[:, :u], total[:, u:])
        for copy in range(parts):
            out_ref[copy] = hidden

    return pl.pallas_call(
        kernel,
        grid=(pieces,),
        out_shape=jax.ShapeDtypeStruct((parts, n, pieces * u), jnp.bfloat16),
        in_specs=[
            pl.BlockSpec((parts, n, k), lambda i: (0, 0, 0)),
            pl.BlockSpec((1, parts * k, both), lambda i: (i, 0, 0)),
        ],
        out_specs=pl.BlockSpec((parts, n, u), lambda i: (0, 0, i)),
        name="gated",
    )(rows, weights)


def lowered(hidden, weights):
    parts, n, k = hidden.shape
    pieces, _, f = weights.shape

    def kernel(hidden_ref, weights_ref, out_ref):
        total = dot(hidden_ref[0], weights_ref[0, :k, :])
        for part in range(1, parts):
            total = total + dot(hidden_ref[part], weights_ref[0, part * k : (part + 1) * k, :])
        out_ref[0] = total.astype(jnp.bfloat16)

    return pl.pallas_call(
        kernel,
        grid=(pieces,),
        out_shape=jax.ShapeDtypeStruct((pieces, n, f), jnp.bfloat16),
        in_specs=[
            pl.BlockSpec((parts, n, k), lambda i: (0, 0, 0)),
            pl.BlockSpec((1, parts * k, f), lambda i: (i, 0, 0)),
        ],
        out_specs=pl.BlockSpec((1, n, f), lambda i: (i, 0, 0)),
        name="lowered",
    )(hidden, weights)


def combine(results, target, logits):
    slots, f = results.shape
    tokens = target.shape[0]

    def kernel(results_ref, target_ref, logits_ref, out_ref):
        chances = jax.nn.softmax(logits_ref[...], axis=-1)
        lane = lax.broadcasted_iota(jnp.int32, (tokens, slots), 1)
        total = jnp.zeros((tokens, f), jnp.float32)
        for k in range(TOP_K):
            chosen = (target_ref[:, k : k + 1] == lane).astype(jnp.float32).astype(jnp.bfloat16)
            total = total + dot(chosen, results_ref[...]) * chances[:, k : k + 1]
        out_ref[...] = total.astype(jnp.bfloat16)

    vmem = pl.BlockSpec(memory_space=pltpu.VMEM)
    return pl.pallas_call(
        kernel,
        out_shape=jax.ShapeDtypeStruct((tokens, f), jnp.bfloat16),
        in_specs=[vmem] * 3,
        out_specs=vmem,
        name="combine",
    )(results, target, logits)


def attention(mixer_input, mixer_gain, query_weight, key_weight, value_weight, sink_logit):
    tokens = mixer_input.shape[0]
    query_heads = query_weight.shape[1] // HEAD_DIM
    key_heads = key_weight.shape[1] // HEAD_DIM
    group = query_heads // key_heads
    blocks = tokens // WINDOW
    offset = lax.axis_index(EP) * tokens
    length = lax.axis_size(EP) * tokens
    places = offset + jnp.arange(tokens, dtype=jnp.int32)
    normed = normalize(mixer_input, mixer_gain)
    query = dot(normed, query_weight).reshape(tokens, query_heads, HEAD_DIM)
    query = (
        axial_rope(query, places)
        .astype(jnp.bfloat16)
        .reshape(blocks, WINDOW, key_heads, group, HEAD_DIM)
    )
    keys = dot(normed, key_weight).reshape(tokens, key_heads, HEAD_DIM)
    keys = axial_rope(keys, places).astype(jnp.bfloat16).reshape(tokens, key_heads * HEAD_DIM)
    values = dot(normed, value_weight).astype(jnp.bfloat16)
    stacked = jnp.concatenate([keys, values], axis=1)
    widened = extended(stacked, EP, WINDOW)
    framed = widened.reshape(blocks + 2, WINDOW, 2, key_heads, HEAD_DIM)
    nearby = jnp.concatenate([framed[:-2], framed[1:-1], framed[2:]], axis=1)
    scores = jnp.einsum(
        "nqgrd,nkgd->ngrqk", query, nearby[:, :, 0], preferred_element_type=jnp.float32
    ) * HEAD_DIM ** (-0.5)
    query_place = places.reshape(blocks, WINDOW)
    key_place = (
        offset
        + (jnp.arange(blocks, dtype=jnp.int32)[:, None] - 1) * WINDOW
        + jnp.arange(3 * WINDOW, dtype=jnp.int32)[None, :]
    )
    allowed = (
        (jnp.abs(query_place[:, :, None] - key_place[:, None, :]) <= WINDOW)
        & (key_place[:, None, :] >= 0)
        & (key_place[:, None, :] < length)
    )
    scores = jnp.where(allowed[:, None, None], scores, -1e30)
    sinks = sink_logit.reshape(key_heads, group)[None, :, :, None]
    top = jnp.maximum(jnp.max(scores, axis=-1), sinks)
    weights = jnp.exp(scores - top[..., None])
    denominator = jnp.sum(weights, axis=-1) + jnp.exp(sinks - top)
    shares = (weights / denominator[..., None]).astype(jnp.bfloat16)
    mixed = jnp.einsum(
        "ngrqk,nkgd->nqgrd", shares, nearby[:, :, 1], preferred_element_type=jnp.float32
    )
    return mixed.astype(jnp.bfloat16).reshape(tokens, query_heads * HEAD_DIM)


def shards(
    mixer_input,
    mixer_gain,
    query_weight,
    key_weight,
    value_weight,
    output_weight,
    sink_logit,
    expert_input,
    expert_gain,
    routes,
    route_logits,
    gate_weight,
    up_weight,
    down_weight,
):
    experts = lax.axis_size(EP)
    rows_here, features = expert_input.shape
    across, along = lax.axis_size("x"), lax.axis_size("y")
    slots = 2 * rows_here * TOP_K // experts // across
    width = features // along
    place = jnp.stack([lax.axis_index("y"), lax.axis_index("x")]).astype(jnp.int32)

    outgoing, target = dispatch(
        expert_input, expert_gain, routes, place, experts, slots, width
    )
    received = swap(outgoing.reshape(experts, slots, width), EP)
    both = spread(jnp.concatenate([gate_weight[0], up_weight[0]], axis=1), "x")
    down = spread(down_weight[0], "x")

    mixed = attention(
        mixer_input, mixer_gain, query_weight, key_weight, value_weight, sink_logit
    )
    heads = spread(mixed, TP)

    rows = spread(received.reshape(experts * slots, width), "y")
    hidden = swap(gated(rows, both), "y")
    result = swap(lowered(hidden, down), "x")
    result = result.reshape(across, experts, slots, -1).transpose(1, 0, 2, 3)
    returned = swap(result, EP)
    expert_output = combine(
        returned.reshape(experts * across * slots, -1), target, route_logits
    )
    pieces = output_weight.reshape(heads.shape[0], heads.shape[2], -1)
    mixer_output = jnp.einsum(
        "trj,tjn->rn", heads, pieces, preferred_element_type=jnp.float32
    ).astype(jnp.bfloat16)
    return (mixer_output, expert_output)


def solution(mesh):
    finer = Mesh(mesh.devices.reshape(16, 2, 4, 4), ("ep_0", "ep_1", "y", "x"))
    in_specs = (
        P(EP, None),
        P(),
        P(None, TP),
        P(None, TP),
        P(None, TP),
        P(None, TP),
        P(TP),
        P(EP, None),
        P(),
        P(EP, None),
        P(EP, None),
        P(EP, None, TP),
        P(EP, None, TP),
        P(EP, None, TP),
    )
    out_specs = (P(EP, TP), P(EP, TP))
    return jax.shard_map(
        shards, mesh=finer, in_specs=in_specs, out_specs=out_specs, check_vma=False
    )
```

time: 255 us -> 234 us (0.918)
  waiting for transfers between devices: 164 us -> 113 us
  blocking collectives: 5.75 us -> 39.1 us
  Pallas kernels: 0 us -> 14.3 us
  between operations: 14.5 us -> 0.99 us
  starting transfers between devices: 34.5 us -> 43.2 us
  matrix products: 13.4 us -> 6.23 us
  other arithmetic: 8.37 us -> 5.1 us
    all_gather x2 -> x0, waiting for transfers between devices: 141 us -> none  [the longest x1 71.7 us: shards(): lax.all_gather(hidden, 'tp', axis=1, tiled=True)]
    all_to_all x2 -> x7, waiting for transfers between devices: 19.2 us -> 113 us  [swap(): return lax.all_to_all(pieces, axis, 0, 0, tiled=True)]
    all_to_all x1, blocking collectives: 5.75 us -> 39.1 us  [swap(): return lax.all_to_all(pieces, axis, 0, 0, tiled=True)]
    pallas_call x0 -> x4, Pallas kernels: none -> 14.3 us  [the longest x1 5.34 us: gated(): pl.pallas_call(kernel, grid=(pieces,), out_shape=jax.ShapeDtypeStruct((pa...]
    all_to_all x2 -> x7, starting transfers between devices: 28.9 us -> 38.2 us  [swap(): return lax.all_to_all(pieces, axis, 0, 0, tiled=True)]
    dot_general x9 -> x6, matrix products: 13.4 us -> 6.23 us  [the longest x3 2.8 us: dot(): return jnp.dot(a, b, preferred_element_type=jnp.float32)]
    broadcast_in_dim x0 -> x6, local copies, waits for them, and re-layouts: none -> 6.51 us  [spread(): jnp.broadcast_to(shard[None], (lax.axis_size(axis), *shard.shape))]
    gather x2 -> x0, local copies, waits for them, and re-layouts: 5.61 us -> none  [the longest x1 4.28 us: shards(): outgoing = own[source].reshape(experts, capacity, width)]
  transfers between devices with their start and end apart: 6 -> 9, of which waited for: 5 -> 7; matrix products, arithmetic and copies ran while one was open for 3% -> 6% of each run, Pallas kernels for 0% -> 2%
where the time goes in v1:
time: 234 us; the launch traced here: 233 us
  waiting for transfers between devices  113 us (48%)
  starting transfers between devices  43.2 us (18%)
  blocking collectives  39.1 us (17%)
  Pallas kernels  14.3 us (6%)
  local copies, waits for them, and re-layouts  11 us (5%)
  matrix products  6.23 us (3%)
  other arithmetic  5.1 us (2%)
    all_to_all x7, waiting for transfers between devices, swap(): return lax.all_to_all(pieces, axis, 0, 0, tiled=True)  113 us
    all_to_all x1, blocking collectives, swap(): return lax.all_to_all(pieces, axis, 0, 0, tiled=True)  39.1 us
    all_to_all x7, starting transfers between devices, swap(): return lax.all_to_all(pieces, axis, 0, 0, tiled=True)  38.2 us
    broadcast_in_dim x6, local copies, waits for them, and re-layouts, spread(): jnp.broadcast_to(shard[None], (lax.axis_size(axis), *shard.shape))  6.51 us
    pallas_call x1, Pallas kernels, gated(): pl.pallas_call(kernel, grid=(pieces,), out_shape=jax.ShapeDtypeStruct((pa...  5.34 us
  transfers between devices with their start and end apart: 9, of which 7 were waited for; matrix products, arithmetic and copies ran while one was open for 6% of the time, Pallas kernels for 2%

profile of v1, /device:TPU:1, one launch (start us, length us, event | category | flops | bytes accessed | tf_op | source)
XLA Modules:
  0.0 232.8 jit_solution(17118837730831385684)
XLA Ops:
  0.6 1.5 copy.33.routes_ref
  2.1 0.6 pad_add_fusion.place_ref
  2.7 2.3 dispatch.1
  5.0 39.1 %all_to_all.40 = bf16[32,8,512]{2,1,0:T(8,128)(2,1)S(1)} all-to-all(bf16[32,8,512]{2,1,0:T(8,128)(2,1)} %bitcast.99), channel_id=1, replica_groups=mesh['ep_0'=16,'ep_1'=2,'y'=4,'x'=4] {'ep_0','ep_1'}, dimensions={0} | all-to-all | bytes 524288 | tf_op jit(solution)/shard_map/all_to_all | solution.py:32
  44.1 1.1 broadcast_in_dim.30
  45.2 4.2 %all-to-all-start.2 = ((bf16[4,256,512]{2,1,0:T(8,128)(2,1)}), bf16[4,256,512]{2,1,0:T(8,128)(2,1)S(1)}, u32[]{:S(2)}, u32[]{:S(2)}) async-start(bf16[4,256,512]{2,1,0:T(8,128)(2,1)} %broadcast_in_dim.30), calls=%async_computation.2 | async-start | bytes 2097152 | tf_op jit(solution)/shard_map/all_to_all | solution.py:32
  49.4 1.2 pad_maximum_fusion
  50.6 13.1 %all-to-all-done.2.rows_ref = bf16[4,256,512]{2,1,0:T(8,128)(2,1)S(1)} async-done(((bf16[4,256,512]{2,1,0:T(8,128)(2,1)}), bf16[4,256,512]{2,1,0:T(8,128)(2,1)S(1)}, u32[]{:S(2)}, u32[]{:S(2)}) %all-to-all-start.2) | async-done | bytes 1048608 | tf_op jit(solution)/shard_map/all_to_all | solution.py:32
  63.7 2.3 %broadcast_in_dim.31 = bf16[4,2048,256]{2,1,0:T(8,128)(2,1)} broadcast(bf16[2048,256]{1,0:T(8,128)(2,1)S(1)} %pad_maximum_fusion), dimensions={1,2} | broadcast | bytes 5242880 | tf_op jit(solution)/shard_map/broadcast_in_dim | solution.py:36
  66.0 5.0 %all-to-all-start.3 = ((bf16[4,2048,256]{2,1,0:T(8,128)(2,1)}), bf16[4,2048,256]{2,1,0:T(8,128)(2,1)}, u32[]{:S(2)}, u32[]{:S(2)}) async-start(bf16[4,2048,256]{2,1,0:T(8,128)(2,1)} %broadcast_in_dim.31), calls=%async_computation.3 | async-start | bytes 8388608 | tf_op jit(solution)/shard_map/all_to_all | solution.py:32
  71.1 0.3 fusion
  71.5 0.5 convolution_bitcast_fusion.1
  72.0 0.1 constant_dynamic-update-slice_fusion.3
  72.1 0.1 constant_dynamic-update-slice_fusion.2
  72.3 0.1 constant_dynamic-update-slice_fusion.1
  72.4 0.1 constant_dynamic-update-slice_fusion
  72.6 0.5 fusion.7
  73.1 2.7 %collective-permute-start = (bf16[128,128]{0,1:T(8,128)(2,1)S(1)}, bf16[128,128]{0,1:T(8,128)(2,1)S(1)}, u32[]{:S(2)}, u32[]{:S(2)}) collective-permute-start(bf16[128,128]{0,1:T(8,128)(2,1)S(1)} %get-tuple-element.15), channel_id=1, source_target_pairs={{0,16},{16,32},{32,48},{48,64},{64,80},{80,96},{96,112},{112,128},... | collective-permute-start | bytes 98312 | tf_op jit(solution)/shard_map/ppermute | solution.py:26
  75.8 2.3 collective-permute-start.1
  78.3 0.2 multiply_cosine_fusion.1
  78.5 39.8 %all-to-all-done.3.weights_ref = bf16[4,2048,256]{2,1,0:T(8,128)(2,1)} async-done(((bf16[4,2048,256]{2,1,0:T(8,128)(2,1)}), bf16[4,2048,256]{2,1,0:T(8,128)(2,1)}, u32[]{:S(2)}, u32[]{:S(2)}) %all-to-all-start.3) | async-done | bytes 4194336 | tf_op jit(solution)/shard_map/all_to_all | solution.py:32
  118.2 1.6 broadcast_in_dim.33
  119.9 3.7 %all-to-all-start.5 = ((bf16[4,2048,128]{2,1,0:T(8,128)(2,1)}), bf16[4,2048,128]{2,1,0:T(8,128)(2,1)S(1)}, u32[]{:S(2)}, u32[]{:S(2)}) async-start(bf16[4,2048,128]{2,1,0:T(8,128)(2,1)} %broadcast_in_dim.33), calls=%async_computation.5 | async-start | bytes 4194304 | tf_op jit(solution)/shard_map/all_to_all | solution.py:32
  123.6 1.8 fusion.45
  125.5 0.5 fusion.11
  126.0 0.6 copy.56
  126.8 5.3 %gated.1 = bf16[4,256,512]{2,1,0:T(8,128)(2,1)} custom-call(bf16[4,256,512]{2,1,0:T(8,128)(2,1)} %copy-done.2, bf16[4,2048,256]{2,1,0:T(8,128)(2,1)} %all-to-all-done.3.weights_ref), custom_call_target="tpu_custom_call" | custom-call | tf_op jit(solution)/shard_map/gated/pallas_call | solution.py:134
  132.1 15.2 %all-to-all-done.5.weights_ref = bf16[4,2048,128]{2,1,0:T(8,128)(2,1)S(1)} async-done(((bf16[4,2048,128]{2,1,0:T(8,128)(2,1)}), bf16[4,2048,128]{2,1,0:T(8,128)(2,1)S(1)}, u32[]{:S(2)}, u32[]{:S(2)}) %all-to-all-start.5) | async-done | bytes 2097184 | tf_op jit(solution)/shard_map/all_to_all | solution.py:32
  147.3 4.2 %all-to-all-start.4 = ((bf16[4,256,512]{2,1,0:T(8,128)(2,1)}), bf16[4,256,512]{2,1,0:T(8,128)(2,1)}, u32[]{:S(2)}, u32[]{:S(2)}) async-start(bf16[4,256,512]{2,1,0:T(8,128)(2,1)} %gated.1), calls=%async_computation.4 | async-start | bytes 2097152 | tf_op jit(solution)/shard_map/all_to_all | solution.py:32
  151.6 1.2 fusion.50
  152.8 0.7 broadcast_maximum_fusion
  153.6 0.1 fusion.8
  153.7 0.7 exponential_add_fusion
  154.4 8.6 %all-to-all-done.4.hidden_ref = bf16[4,256,512]{2,1,0:T(8,128)(2,1)} async-done(((bf16[4,256,512]{2,1,0:T(8,128)(2,1)}), bf16[4,256,512]{2,1,0:T(8,128)(2,1)}, u32[]{:S(2)}, u32[]{:S(2)}) %all-to-all-start.4) | async-done | bytes 1048608 | tf_op jit(solution)/shard_map/all_to_all | solution.py:32
  163.1 4.6 %lowered.1 = bf16[4,256,128]{2,1,0:T(8,128)(2,1)} custom-call(bf16[4,256,512]{2,1,0:T(8,128)(2,1)} %all-to-all-done.4.hidden_ref, bf16[4,2048,128]{2,1,0:T(8,128)(2,1)} %copy-done.1), custom_call_target="tpu_custom_call" | custom-call | tf_op jit(solution)/shard_map/lowered/pallas_call | solution.py:157
  167.6 3.4 %all-to-all-start.6 = ((bf16[4,256,128]{2,1,0:T(8,128)(2,1)}), bf16[4,256,128]{2,1,0:T(8,128)(2,1)S(1)}, u32[]{:S(2)}, u32[]{:S(2)}) async-start(bf16[4,256,128]{2,1,0:T(8,128)(2,1)} %lowered.1), calls=%async_computation.6 | async-start | bytes 524288 | tf_op jit(solution)/shard_map/all_to_all | solution.py:32
  171.0 1.2 fusion.6
  172.4 4.1 %all-to-all-done.6 = bf16[4,256,128]{2,1,0:T(8,128)(2,1)S(1)} async-done(((bf16[4,256,128]{2,1,0:T(8,128)(2,1)}), bf16[4,256,128]{2,1,0:T(8,128)(2,1)S(1)}, u32[]{:S(2)}, u32[]{:S(2)}) %all-to-all-start.6) | async-done | bytes 262176 | tf_op jit(solution)/shard_map/all_to_all | solution.py:32
  176.5 1.2 broadcast_in_dim.27
  177.7 3.7 %all-to-all-start = ((bf16[16,256,128]{2,1,0:T(8,128)(2,1)}), bf16[16,256,128]{2,1,0:T(8,128)(2,1)S(1)}, u32[]{:S(2)}, u32[]{:S(2)}) async-start(bf16[16,256,128]{2,1,0:T(8,128)(2,1)} %broadcast_in_dim.27), calls=%async_computation | async-start | bytes 2097152 | tf_op jit(solution)/shard_map/all_to_all | solution.py:32
  181.4 0.8 copy_bitcast_fusion
  182.1 11.6 %all-to-all-done = bf16[16,256,128]{2,1,0:T(8,128)(2,1)S(1)} async-done(((bf16[16,256,128]{2,1,0:T(8,128)(2,1)}), bf16[16,256,128]{2,1,0:T(8,128)(2,1)S(1)}, u32[]{:S(2)}, u32[]{:S(2)}) %all-to-all-start) | async-done | bytes 1048608 | tf_op jit(solution)/shard_map/all_to_all | solution.py:32
  193.7 14.0 %all-to-all-start.7 = ((bf16[32,4,8,128]{3,2,1,0:T(8,128)(2,1)}), bf16[32,4,8,128]{3,2,1,0:T(8,128)(2,1)S(1)}, u32[]{:S(2)}, u32[]{:S(2)}) async-start(bf16[32,4,8,128]{3,2,1,0:T(8,128)(2,1)} %copy_bitcast_fusion), calls=%async_computation.7 | async-start | bytes 524288 | tf_op jit(solution)/shard_map/all_to_all | solution.py:32
  207.7 0.7 copy.35.logits_ref
  208.5 1.1 fusion.5
  209.5 20.5 %all-to-all-done.7 = bf16[32,4,8,128]{3,2,1,0:T(8,128)(2,1)S(1)} async-done(((bf16[32,4,8,128]{3,2,1,0:T(8,128)(2,1)}), bf16[32,4,8,128]{3,2,1,0:T(8,128)(2,1)S(1)}, u32[]{:S(2)}, u32[]{:S(2)}) %all-to-all-start.7) | async-done | bytes 262176 | tf_op jit(solution)/shard_map/all_to_all | solution.py:32
  230.0 0.7 copy-done.4
  230.7 2.1 combine.1
  (48 shorter events, 0.7 us)
Async XLA Ops:
  0.6 207.8 %copy-start = (bf16[2048,128]{1,0:T(8,128)(2,1)S(1)}, bf16[2048,128]{1,0:T(8,128)(2,1)}, u32[]{:S(2)}) copy-start(bf16[2048,128]{1,0:T(8,128)(2,1)} %param.19) | copy-start | bytes 1572868
  5.0 44.4 %copy-start.6 = (bf16[1,2048,128]{2,1,0:T(8,128)(2,1)S(1)}, bf16[1,2048,128]{2,1,0:T(8,128)(2,1)}, u32[]{:S(2)}) copy-start(bf16[1,2048,128]{2,1,0:T(8,128)(2,1)} %param.26) | copy-start | bytes 1572868
  45.2 18.4 %all-to-all-start.2 = ((bf16[4,256,512]{2,1,0:T(8,128)(2,1)}), bf16[4,256,512]{2,1,0:T(8,128)(2,1)S(1)}, u32[]{:S(2)}, u32[]{:S(2)}) async-start(bf16[4,256,512]{2,1,0:T(8,128)(2,1)} %broadcast_in_dim.30), calls=%async_computation.2 | async-start | bytes 2097152 | tf_op jit(solution)/shard_map/all_to_all | solution.py:32
  63.7 2.3 %copy-start.2 = (bf16[4,256,512]{2,1,0:T(8,128)(2,1)}, bf16[4,256,512]{2,1,0:T(8,128)(2,1)S(1)}, u32[]{:S(2)}) copy-start(bf16[4,256,512]{2,1,0:T(8,128)(2,1)S(1)} %all-to-all-done.2.rows_ref) | copy-start | bytes 3145732
  66.0 5.1 %copy-start.3 = (bf16[256,2048]{1,0:T(8,128)(2,1)S(1)}, bf16[256,2048]{1,0:T(8,128)(2,1)}, u32[]{:S(2)}) copy-start(bf16[256,2048]{1,0:T(8,128)(2,1)} %param.14) | copy-start | bytes 3145732
  66.0 5.4 %copy-start.10 = (bf16[2048,64]{0,1:T(8,128)(2,1)S(1)}, bf16[2048,64]{0,1:T(8,128)(2,1)}, u32[]{:S(2)}) copy-start(bf16[2048,64]{0,1:T(8,128)(2,1)} %param.17) | copy-start | bytes 786436
  66.0 5.4 %copy-start.12 = (f32[2048]{0:T(1024)S(1)}, f32[2048]{0:T(1024)}, u32[]{:S(2)}) copy-start(f32[2048]{0:T(1024)} %param.15) | copy-start | bytes 24580
  66.0 52.2 %all-to-all-start.3 = ((bf16[4,2048,256]{2,1,0:T(8,128)(2,1)}), bf16[4,2048,256]{2,1,0:T(8,128)(2,1)}, u32[]{:S(2)}, u32[]{:S(2)}) async-start(bf16[4,2048,256]{2,1,0:T(8,128)(2,1)} %broadcast_in_dim.31), calls=%async_computation.3 | async-start | bytes 8388608 | tf_op jit(solution)/shard_map/all_to_all | solution.py:32
  71.1 1.5 copy-start.11
  71.4 46.8 %copy-start.5 = (bf16[1,2048,128]{2,1,0:T(8,128)(2,1)S(1)}, bf16[1,2048,128]{2,1,0:T(8,128)(2,1)}, u32[]{:S(2)}) copy-start(bf16[1,2048,128]{2,1,0:T(8,128)(2,1)} %param.27) | copy-start | bytes 1572868
  73.1 53.5 %collective-permute-start = (bf16[128,128]{0,1:T(8,128)(2,1)S(1)}, bf16[128,128]{0,1:T(8,128)(2,1)S(1)}, u32[]{:S(2)}, u32[]{:S(2)}) collective-permute-start(bf16[128,128]{0,1:T(8,128)(2,1)S(1)} %get-tuple-element.15), channel_id=1, source_target_pairs={{0,16},{16,32},{32,48},{48,64},{64,80},{80,96},{96,112},{112,128},... | collective-permute-start | bytes 98312 | tf_op jit(solution)/shard_map/ppermute | solution.py:26
  75.8 50.8 %collective-permute-start.1 = (bf16[128,128]{0,1:T(8,128)(2,1)S(1)}, bf16[128,128]{0,1:T(8,128)(2,1)S(1)}, u32[]{:S(2)}, u32[]{:S(2)}) collective-permute-start(bf16[128,128]{0,1:T(8,128)(2,1)S(1)} %get-tuple-element.14), channel_id=1, source_target_pairs={{16,0},{32,16},{48,32},{64,48},{80,64},{96,80},{112,96},{128,112},... | collective-permute-start | bytes 98312 | tf_op jit(solution)/shard_map/ppermute | solution.py:27
  119.9 3.8 %copy-start.9 = (bf16[2048,128]{1,0:T(8,128)(2,1)S(1)}, bf16[2048,128]{1,0:T(8,128)(2,1)}, u32[]{:S(2)}) copy-start(bf16[2048,128]{1,0:T(8,128)(2,1)} %param.16) | copy-start | bytes 1572868
  119.9 27.5 %all-to-all-start.5 = ((bf16[4,2048,128]{2,1,0:T(8,128)(2,1)}), bf16[4,2048,128]{2,1,0:T(8,128)(2,1)S(1)}, u32[]{:S(2)}, u32[]{:S(2)}) async-start(bf16[4,2048,128]{2,1,0:T(8,128)(2,1)} %broadcast_in_dim.33), calls=%async_computation.5 | async-start | bytes 4194304 | tf_op jit(solution)/shard_map/all_to_all | solution.py:32
  126.8 5.4 %copy-start.7 = (bf16[2,384,2,1,64]{1,4,0,3,2:T(8,128)(2,1)}, bf16[2,384,2,1,64]{1,4,0,3,2:T(8,128)(2,1)S(1)}, u32[]{:S(2)}) copy-start(bf16[2,384,2,1,64]{1,4,0,3,2:T(8,128)(2,1)S(1)} %copy_dynamic-update-slice_fusion) | copy-start | bytes 589828
  147.3 15.7 %copy-start.1 = (bf16[4,2048,128]{2,1,0:T(8,128)(2,1)}, bf16[4,2048,128]{2,1,0:T(8,128)(2,1)S(1)}, u32[]{:S(2)}) copy-start(bf16[4,2048,128]{2,1,0:T(8,128)(2,1)S(1)} %all-to-all-done.5.weights_ref) | copy-start | bytes 6291460
  147.3 15.7 %all-to-all-start.4 = ((bf16[4,256,512]{2,1,0:T(8,128)(2,1)}), bf16[4,256,512]{2,1,0:T(8,128)(2,1)}, u32[]{:S(2)}, u32[]{:S(2)}) async-start(bf16[4,256,512]{2,1,0:T(8,128)(2,1)} %gated.1), calls=%async_computation.4 | async-start | bytes 2097152 | tf_op jit(solution)/shard_map/all_to_all | solution.py:32
  167.6 8.9 %all-to-all-start.6 = ((bf16[4,256,128]{2,1,0:T(8,128)(2,1)}), bf16[4,256,128]{2,1,0:T(8,128)(2,1)S(1)}, u32[]{:S(2)}, u32[]{:S(2)}) async-start(bf16[4,256,128]{2,1,0:T(8,128)(2,1)} %lowered.1), calls=%async_computation.6 | async-start | bytes 524288 | tf_op jit(solution)/shard_map/all_to_all | solution.py:32
  172.4 35.3 %copy-start.8 = (f32[128,4]{0,1:T(4,128)S(1)}, f32[128,4]{0,1:T(4,128)}, u32[]{:S(2)}) copy-start(f32[128,4]{0,1:T(4,128)} %param.24) | copy-start | bytes 6148
  177.7 16.0 %all-to-all-start = ((bf16[16,256,128]{2,1,0:T(8,128)(2,1)}), bf16[16,256,128]{2,1,0:T(8,128)(2,1)S(1)}, u32[]{:S(2)}, u32[]{:S(2)}) async-start(bf16[16,256,128]{2,1,0:T(8,128)(2,1)} %broadcast_in_dim.27), calls=%async_computation | async-start | bytes 2097152 | tf_op jit(solution)/shard_map/all_to_all | solution.py:32
  193.7 36.3 %all-to-all-start.7 = ((bf16[32,4,8,128]{3,2,1,0:T(8,128)(2,1)}), bf16[32,4,8,128]{3,2,1,0:T(8,128)(2,1)S(1)}, u32[]{:S(2)}, u32[]{:S(2)}) async-start(bf16[32,4,8,128]{3,2,1,0:T(8,128)(2,1)} %copy_bitcast_fusion), calls=%async_computation.7 | async-start | bytes 524288 | tf_op jit(solution)/shard_map/all_to_all | solution.py:32
  230.0 0.7 copy-start.4
